TPU v7x, 32 devices: a whole 2x2x4 slice. The times are simulated.
32 devices in a mesh: sp: 8 (over z, x), tp: 4 (over y, core).
Axes of the slice: x: 2, y: 2, z: 4, core: 2. Of those that a mesh axis runs over, the one named last changes fastest.
Arguments:
- queries: bfloat16 [4096, 2048], P('sp', 'tp'), may hold values from -90 to 90, as said below
- key_rows: bfloat16 [4096, 512], P('sp', 'tp'), may hold values from -6 to 6
- value_rows: bfloat16 [4096, 512], P('sp', 'tp'), may hold values from -6 to 6
- sink_logits: float32 [16], P('tp'), may hold values from 2 to 7
- residual: bfloat16 [4096, 2048], P('sp'), may hold values from -6 to 6
- norm_gain: float32 [2048], replicated, may hold values from 0.1 to 1.9
- out_weight: bfloat16 [2048, 2048], P('tp'), may hold values from -1.5 to 1.5
- gate_weight: bfloat16 [2048, 5632], P('sp', 'tp'), may hold values from -0.125 to 0.125
- up_weight: bfloat16 [2048, 5632], P('sp', 'tp'), may hold values from -0.125 to 0.125
- down_weight: bfloat16 [5632, 2048], P('tp', 'sp'), may hold values from -0.078125 to 0.078125
Outputs:
- mixed: bfloat16 [4096, 2048], P(('sp', 'tp'))
Inputs may be any that keep to these rules, and one draw needn't show every extreme that they name: queries are mostly of order one; some rows may be much larger.
All inputs are finite; a program needn't handle non-finite values.
Results may differ from a plain program's by a relative error of at most 0.012.
Values may be sent and summed in bfloat16 or wider, within the bound.
A program may use at most 128 MiB of HBM per device.

v0:
```python
import jax
import jax.numpy as jnp
from jax import lax
from jax.sharding import PartitionSpec as P

DH = 128
WIN = 128
EPSILON = 1e-06
MASKED = -1e30


def with_halo(cells, sides, width):
    for axis, dim in sides:
        count = lax.axis_size(axis)
        ends = count - 1
        head = lax.slice_in_dim(cells, 0, width, axis=dim)
        tail = lax.slice_in_dim(cells, cells.shape[dim] - width, cells.shape[dim], axis=dim)
        cells = jnp.concatenate(
            [
                lax.ppermute(tail, axis, [(i, (i + 1) % count) for i in range(ends)]),
                cells,
                lax.ppermute(head, axis, [((i + 1) % count, i) for i in range(ends)]),
            ],
            axis=dim,
        )
    return cells


def attend_block(query_blk, key_blk, value_blk, sink_logits, query_pos, key_pos, seq_len):
    kv_heads = key_blk.shape[1] // DH
    group_size = query_blk.shape[1] // key_blk.shape[1]
    query_four = query_blk.reshape(query_blk.shape[0], kv_heads, group_size, DH)
    key_three = key_blk.reshape(key_blk.shape[0], kv_heads, DH)
    value_three = value_blk.reshape(value_blk.shape[0], kv_heads, DH)
    scores = jnp.einsum(
        "qhgd,khd->hgqk", query_four, key_three, preferred_element_type=jnp.float32
    ) * DH ** (-0.5)
    allowed = (
        (jnp.abs(key_pos[None, :] - query_pos[:, None]) <= WIN)
        & (key_pos[None, :] >= 0)
        & (key_pos[None, :] < seq_len)
    )
    scores = jnp.where(allowed[None, None], scores, MASKED)
    sink_col = sink_logits.reshape(kv_heads, group_size)[:, :, None]
    highest = jnp.maximum(jnp.max(scores, axis=-1), sink_col)
    weights_exp = jnp.exp(scores - highest[..., None])
    denominator = jnp.sum(weights_exp, axis=-1) + jnp.exp(sink_col - highest)
    probabilities = (weights_exp / denominator[..., None]).astype(jnp.bfloat16)
    heads_out = jnp.einsum(
        "hgqk,khd->qhgd", probabilities, value_three, preferred_element_type=jnp.float32
    )
    return heads_out.astype(jnp.bfloat16).reshape(query_blk.shape[0], kv_heads * group_size * DH)


def rms_scale(rows_wide, norm_gain):
    mean_square = jnp.mean(rows_wide * rows_wide, axis=-1, keepdims=True)
    return (rows_wide * lax.rsqrt(mean_square + EPSILON) * norm_gain).astype(jnp.bfloat16)


def fetch_down(down_weight):
    return lax.all_gather(down_weight, "sp", axis=1, tiled=True)


def shards(
    queries,
    key_rows,
    value_rows,
    sink_logits,
    residual,
    norm_gain,
    out_weight,
    gate_weight,
    up_weight,
    down_weight,
):
    tok_local = queries.shape[0]
    block_len = 2 * WIN
    share_rows = tok_local // lax.axis_size("tp")
    seq_len = tok_local * lax.axis_size("sp")
    device_offset = lax.axis_index("sp") * tok_local
    kv_pair = jnp.stack([key_rows, value_rows])
    kv_ext = with_halo(kv_pair, (("sp", 1),), WIN)

    def one_block(block_index):
        block_first = block_index * block_len
        query_blk = lax.dynamic_slice_in_dim(queries, block_first, block_len, 0)
        key_blk = lax.dynamic_slice_in_dim(kv_ext[0], block_first, block_len + 2 * WIN, 0)
        value_blk = lax.dynamic_slice_in_dim(kv_ext[1], block_first, block_len + 2 * WIN, 0)
        query_pos = device_offset + block_first + jnp.arange(block_len, dtype=jnp.int32)
        key_pos = (
            device_offset + block_first - WIN + jnp.arange(block_len + 2 * WIN, dtype=jnp.int32)
        )
        return attend_block(query_blk, key_blk, value_blk, sink_logits, query_pos, key_pos, seq_len)

    blocks = lax.map(one_block, jnp.arange(tok_local // block_len, dtype=jnp.int32))
    attended = blocks.reshape(tok_local, queries.shape[1])
    own_first = lax.axis_index("tp") * share_rows
    attn_full = lax.psum(
        jnp.dot(attended, out_weight, preferred_element_type=jnp.float32).astype(jnp.bfloat16), "tp"
    ).astype(jnp.float32)
    middle_all = residual.astype(jnp.float32) + attn_full
    normed_all = rms_scale(middle_all, norm_gain)
    middle_own = lax.dynamic_slice_in_dim(middle_all, own_first, share_rows, 0)
    gate_sectioned = lax.all_gather(gate_weight, "sp", axis=0, tiled=True)
    up_sectioned = lax.all_gather(up_weight, "sp", axis=0, tiled=True)
    gate_acc = jnp.dot(normed_all, gate_sectioned, preferred_element_type=jnp.float32)
    up_acc = jnp.dot(normed_all, up_sectioned, preferred_element_type=jnp.float32)
    down_whole = fetch_down(down_weight)
    hidden = (jax.nn.silu(gate_acc) * up_acc).astype(jnp.bfloat16)
    ffn_share = lax.psum_scatter(
        jnp.dot(hidden, down_whole, preferred_element_type=jnp.float32).astype(jnp.bfloat16),
        "tp",
        scatter_dimension=0,
        tiled=True,
    ).astype(jnp.float32)
    return (middle_own + ffn_share).astype(jnp.bfloat16)


def solution(mesh):
    placed = (
        P("sp", "tp"),
        P("sp", "tp"),
        P("sp", "tp"),
        P("tp"),
        P("sp", None),
        P(),
        P("tp", None),
        P("sp", "tp"),
        P("sp", "tp"),
        P("tp", "sp"),
    )
    return jax.shard_map(
        shards, mesh=mesh, in_specs=placed, out_specs=P(("sp", "tp"), None), check_vma=False
    )
```

profile of v0, /device:TPU:0, one launch (start us, length us, event | category | flops | bytes accessed | tf_op | source)
XLA Modules:
  0.0 370.6 jit_solution(8707252518556242722)
XLA Ops:
  7.4 1.0 pad_maximum_fusion.2
  8.3 4.9 %collective-permute-start = (bf16[2,128,128]{2,1,0:T(8,128)(2,1)S(1)}, bf16[2,128,128]{2,1,0:T(8,128)(2,1)S(1)}, u32[]{:S(2)}, u32[]{:S(2)}) collective-permute-start(bf16[2,128,128]{2,1,0:T(8,128)(2,1)S(1)} %get-tuple-element.124), channel_id=1, source_target_pairs={{0,4},{4,8},{8,12},{12,16},{16,20},{20,24},{24,28},{1,5},{5,9},{9,... | collective-permute-start | bytes 196616 | tf_op jit(solution)/shard_map/ppermute | solution.py:20
  13.2 1.3 collective-permute-start.1
  14.5 0.6 collective-permute-done
  15.1 4.3 %collective-permute-done.1 = bf16[2,128,128]{2,1,0:T(8,128)(2,1)S(1)} collective-permute-done((bf16[2,128,128]{2,1,0:T(8,128)(2,1)S(1)}, bf16[2,128,128]{2,1,0:T(8,128)(2,1)S(1)}, u32[]{:S(2)}, u32[]{:S(2)}) %collective-permute-start.1) | collective-permute-done | bytes 65568 | tf_op jit(solution)/shard_map/ppermute | solution.py:22
  19.4 1.0 pad_maximum_fusion
  20.4 11.1 %while.12 = (s32[]{:T(128)}, bf16[2,256,512]{2,1,0:T(8,128)(2,1)}, bf16[2,768,128]{2,1,0:T(8,128)(2,1)S(1)}, s32[2]{0:T(128)S(1)}, s32[]{:T(128)}, /*index=5*/bf...) while((s32[]{:T(128)}, bf16[2,256,512]{2,1,0:T(8,128)(2,1)}, ...), condition=%wide.region_3.4_spmd, body=%wide.region_0.3_spmd.sunk | while | flops 273420544 | bytes 14467512 | solution.py:95
  20.4 0.6 dynamic_slice.42
  22.0 1.0 constant_dynamic-slice_fusion.2
  24.1 0.5 convolution_convert_fusion.4
  25.2 0.8 copy-done.3
  26.0 0.6 dynamic_slice.42
  27.6 1.0 constant_dynamic-slice_fusion.2
  30.7 0.8 copy-done.3
  31.5 3.6 convolution_convert_fusion.1
  37.0 50.9 %all-reduce.2.cloned.1.call-done = bf16[512,2048]{1,0:T(8,128)(2,1)} async-done(((bf16[512,2048]{1,0:T(8,128)(2,1)}), bf16[512,2048]{1,0:T(8,128)(2,1)}) %all-reduce.2.cloned.1.call-update) | async-done | bytes 2097168 | tf_op jit(solution)/shard_map/psum | solution.py:98
  87.9 4.9 %convert_add_fusion = (f32[512,2048]{1,0:T(8,128)}, f32[512]{0:T(512)S(1)}) fusion(bf16[512,2048]{1,0:T(8,128)(2,1)} %all-reduce.2.cloned.1.call-done, bf16[512,2048]{1,0:T(8,128)(2,1)} %param.16), kind=kLoop, calls=%fused_computation.25 | loop fusion | flops 5242368 | bytes 8390656 | tf_op jit(solution)/shard_map/add | solution.py:101
  92.8 38.4 %all-gather.4.cloned.1.call-done = bf16[2048,1408]{1,0:T(8,128)(2,1)} async-done(((bf16[256,1408]{1,0:T(8,128)(2,1)}), bf16[2048,1408]{1,0:T(8,128)(2,1)}) %all-gather.4.cloned.1.call-update) | async-done | bytes 5767184 | tf_op jit(solution)/shard_map/all_gather | solution.py:104
  131.2 9.0 %fusion.14 = f32[512,1408]{1,0:T(8,128)} fusion(bf16[2048,1408]{1,0:T(8,128)(2,1)} %all-gather.4.cloned.1.call-done, f32[2048]{0:T(1024)S(1)} %copy-done.4, f32[512]{0:T(512)S(1)} %add_rsqrt_fusion, bf16[512,2048]{1,0:T(8,128)(2,1)} %all-reduce.2.cloned.1.call-done, bf16[512,2048]{1,0:T(8,128)(2,1)} %param.16), kind=kOutput, calls=%fused_computation.36 | convolution fusion | flops 2959081472 | bytes 12855296 | tf_op jit(solution)/shard_map/dot_general | solution.py:106
  140.2 83.4 %all-gather.6.cloned.1.call-done = bf16[2048,1408]{1,0:T(8,128)(2,1)} async-done(((bf16[256,1408]{1,0:T(8,128)(2,1)}), bf16[2048,1408]{1,0:T(8,128)(2,1)}) %all-gather.6.cloned.1.call-update) | async-done | bytes 5767184 | tf_op jit(solution)/shard_map/all_gather | solution.py:105
  223.6 93.0 %all-gather.8.cloned.1.call-done = bf16[1408,2048]{1,0:T(8,128)(2,1)} async-done(((bf16[1408,256]{1,0:T(8,128)(2,1)}), bf16[1408,2048]{1,0:T(8,128)(2,1)}) %all-gather.8.cloned.1.call-update) | async-done | bytes 5767184 | tf_op jit(solution)/shard_map/all_gather | solution.py:61
  316.5 14.6 %convolution_convert_fusion.2 = bf16[512,2048]{1,0:T(8,128)(2,1)} fusion(bf16[1408,2048]{1,0:T(8,128)(2,1)} %all-gather.8.cloned.1.call-done, bf16[2048,1408]{1,0:T(8,128)(2,1)} %all-gather.6.cloned.1.call-done, f32[512,1408]{1,0:T(8,128)} %fusion.14, f32[2048]{0:T(1024)S(1)} %copy-done.4, f32[512]{0:T(512)S(1)} %add_rsqrt_fusion, ...), kind=kOutput, calls=%fused_computation.29 | convolution fusion | flops 5917245440 | bytes 20719616 | tf_op jit(solution)/shard_map/dot_general | solution.py:111
  331.2 29.5 %reduce-scatter.2.cloned.1.call-done = bf16[128,2048]{1,0:T(8,128)(2,1)} async-done(((bf16[512,2048]{1,0:T(8,128)(2,1)}), bf16[128,2048]{1,0:T(8,128)(2,1)}) %reduce-scatter.2.cloned.1.call-update) | async-done | bytes 524304 | tf_op jit(solution)/shard_map/reduce_scatter | solution.py:110
  360.7 2.3 add_convert_fusion
  (52 shorter events, 6.1 us)
Async XLA Ops:
  7.4 24.2 %copy-start = (bf16[512,2048]{1,0:T(8,128)(2,1)S(1)}, bf16[512,2048]{1,0:T(8,128)(2,1)}, u32[]{:S(2)}) copy-start(bf16[512,2048]{1,0:T(8,128)(2,1)} %param.18) | copy-start | bytes 6291460
  7.4 80.6 %all-reduce.2.cloned.1.call-start = ((), (), s32[]{:S(2)}) async-start(), calls=%async_computation.1 | async-start | bytes 4194304 | tf_op jit(solution)/shard_map/psum | solution.py:98
  8.3 6.8 %collective-permute-start = (bf16[2,128,128]{2,1,0:T(8,128)(2,1)S(1)}, bf16[2,128,128]{2,1,0:T(8,128)(2,1)S(1)}, u32[]{:S(2)}, u32[]{:S(2)}) collective-permute-start(bf16[2,128,128]{2,1,0:T(8,128)(2,1)S(1)} %get-tuple-element.124), channel_id=1, source_target_pairs={{0,4},{4,8},{8,12},{12,16},{16,20},{20,24},{24,28},{1,5},{5,9},{9,... | collective-permute-start | bytes 196616 | tf_op jit(solution)/shard_map/ppermute | solution.py:20
  13.2 6.2 %collective-permute-start.1 = (bf16[2,128,128]{2,1,0:T(8,128)(2,1)S(1)}, bf16[2,128,128]{2,1,0:T(8,128)(2,1)S(1)}, u32[]{:S(2)}, u32[]{:S(2)}) collective-permute-start(bf16[2,128,128]{2,1,0:T(8,128)(2,1)S(1)} %get-tuple-element.125), channel_id=1, source_target_pairs={{4,0},{8,4},{12,8},{16,12},{20,16},{24,20},{28,24},{5,1},{9,5},{13... | collective-permute-start | bytes 196616 | tf_op jit(solution)/shard_map/ppermute | solution.py:22
  20.4 3.2 copy-start.1
  24.1 1.0 copy-start.2
  25.2 0.8 copy-start.3
  26.0 3.2 copy-start.1
  29.7 1.0 copy-start.2
  30.7 0.8 copy-start.3
  35.2 96.0 %all-gather.4.cloned.1.call-start = ((), (), s32[]{:S(2)}) async-start(), calls=%async_computation.2 | async-start | bytes 6488064 | tf_op jit(solution)/shard_map/all_gather | solution.py:104
  35.8 187.8 %all-gather.6.cloned.1.call-start = ((), (), s32[]{:S(2)}) async-start(), calls=%async_computation.3 | async-start | bytes 6488064 | tf_op jit(solution)/shard_map/all_gather | solution.py:105
  36.4 280.2 %all-gather.8.cloned.1.call-start = ((), (), s32[]{:S(2)}) async-start(), calls=%async_computation.4 | async-start | bytes 6488064 | tf_op jit(solution)/shard_map/all_gather | solution.py:61
  37.0 94.3 %copy-start.4 = (f32[2048]{0:T(1024)S(1)}, f32[2048]{0:T(1024)}, u32[]{:S(2)}) copy-start(f32[2048]{0:T(1024)} %param.17) | copy-start | bytes 24580
  37.0 323.7 %reduce-scatter.2.cloned.1.call-start = ((), (), s32[]{:S(2)}) async-start(), calls=%async_computation.5 | async-start | bytes 2621440 | tf_op jit(solution)/shard_map/reduce_scatter | solution.py:110
Sparse Core Ops, SparseCore 0:
  35.3 52.5 all-reduce.1
  331.3 29.3 reduce-scatter.1
Sparse Core Ops, SparseCore 1:
  37.9 93.3 all-gather.3
  133.3 90.2 all-gather.5
  225.5 91.0 all-gather.7
where the time goes:
time: 371 us
  waiting for transfers between devices  302 us (81%)
  matrix products  29.2 us (8%)
  between operations  15.1 us (4%)
  other arithmetic  10.6 us (3%)
  starting transfers between devices  6.34 us (2%)
  local copies, waits for them, and re-layouts  6.13 us (2%)
    all_gather x1, waiting for transfers between devices, fetch_down(): return lax.all_gather(down_weight, 'sp', axis=1, tiled=True)  93 us
    all_gather x1, waiting for transfers between devices, shards(): up_sectioned = lax.all_gather(up_weight, 'sp', axis=0, tiled=True)  83.4 us
    psum x1, waiting for transfers between devices, shards(): lax.psum(jnp.dot(attended, out_weight, preferred_element_type=jnp.float32...  50.9 us
    all_gather x1, waiting for transfers between devices, shards(): gate_sectioned = lax.all_gather(gate_weight, 'sp', axis=0, tiled=True)  38.4 us
    reduce_scatter x1, waiting for transfers between devices, shards(): lax.psum_scatter(jnp.dot(hidden, down_whole, preferred_element_type=jnp.f...  29.5 us
    dot_general x1, matrix products, shards(): jnp.dot(hidden, down_whole, preferred_element_type=jnp.float32)  14.6 us
    dot_general x1, matrix products, shards(): jnp.dot(normed_all, gate_sectioned, preferred_element_type=jnp.float32)  8.96 us
  transfers between devices with their start and end apart: 7, of which 7 were waited for; matrix products, arithmetic and copies ran while one was open for 4% of the time, Pallas kernels for 0%

commit v1 on v0

--- a/solution.py
+++ b/solution.py
@@ -101,7 +101,12 @@
     middle_all = residual.astype(jnp.float32) + attn_full
     normed_all = rms_scale(middle_all, norm_gain)
     middle_own = lax.dynamic_slice_in_dim(middle_all, own_first, share_rows, 0)
-    gate_sectioned = lax.all_gather(gate_weight, "sp", axis=0, tiled=True)
+    ring = [gate_weight]
+    for hop in range(7):
+        ring.append(lax.ppermute(ring[-1], "sp", [(dev, (dev + 1) % 8) for dev in range(8)]))
+    gate_sectioned = jnp.roll(
+        jnp.concatenate(ring[::-1], axis=0), (lax.axis_index("sp") + 1) * ring[0].shape[0], axis=0
+    )
     up_sectioned = lax.all_gather(up_weight, "sp", axis=0, tiled=True)
     gate_acc = jnp.dot(normed_all, gate_sectioned, preferred_element_type=jnp.float32)
     up_acc = jnp.dot(normed_all, up_sectioned, preferred_element_type=jnp.float32)

time: 371 us -> 365 us (0.984)
  waiting for transfers between devices: 302 us -> 265 us
  local copies, waits for them, and re-layouts: 6.13 us -> 29.1 us
  starting transfers between devices: 6.34 us -> 13.4 us
    ppermute x0 -> x7, waiting for transfers between devices: none -> 191 us  [shards(): lax.ppermute(ring[-1], 'sp', [(dev, (dev + 1) % 8) for dev in range(8)])]
    all_gather x1, waiting for transfers between devices: 83.4 us -> 0.01 us  [shards(): up_sectioned = lax.all_gather(up_weight, 'sp', axis=0, tiled=True)]
    all_gather x1, waiting for transfers between devices: 93 us -> 18.7 us  [fetch_down(): return lax.all_gather(down_weight, 'sp', axis=1, tiled=True)]
    psum x1, waiting for transfers between devices: 50.9 us -> 0.01 us  [shards(): lax.psum(jnp.dot(attended, out_weight, preferred_element_type=jnp.float32...]
    all_gather x1 -> x0, waiting for transfers between devices: 38.4 us -> none  [shards(): gate_sectioned = lax.all_gather(gate_weight, 'sp', axis=0, tiled=True)]
    unnamed x4 -> x41, local copies, waits for them, and re-layouts: 0.01 us -> 22.9 us
    reduce_scatter x1, waiting for transfers between devices: 29.5 us -> 49.2 us  [shards(): lax.psum_scatter(jnp.dot(hidden, down_whole, preferred_element_type=jnp.f...]
    ppermute x0 -> x7, starting transfers between devices: none -> 7.14 us  [shards(): lax.ppermute(ring[-1], 'sp', [(dev, (dev + 1) % 8) for dev in range(8)])]
  transfers between devices with their start and end apart: 7 -> 13, of which waited for: 7 -> 11; matrix products, arithmetic and copies ran while one was open for 4% -> 9% of each run, Pallas kernels for 0% -> 0%
where the time goes in v1:
time: 365 us; the launch traced here: 364 us
  waiting for transfers between devices  265 us (73%)
  matrix products  29.4 us (8%)
  local copies, waits for them, and re-layouts  29.1 us (8%)
  between operations  15 us (4%)
  starting transfers between devices  13.4 us (4%)
  other arithmetic  10.8 us (3%)
    ppermute x7, waiting for transfers between devices, shards(): lax.ppermute(ring[-1], 'sp', [(dev, (dev + 1) % 8) for dev in range(8)])  191 us
    reduce_scatter x1, waiting for transfers between devices, shards(): lax.psum_scatter(jnp.dot(hidden, down_whole, preferred_element_type=jnp.f...  49.2 us
    unnamed x41, local copies, waits for them, and re-layouts  22.9 us
    all_gather x1, waiting for transfers between devices, fetch_down(): return lax.all_gather(down_weight, 'sp', axis=1, tiled=True)  18.7 us
    dot_general x1, matrix products, shards(): jnp.dot(hidden, down_whole, preferred_element_type=jnp.float32)  14.6 us
    dot_general x1, matrix products, shards(): jnp.dot(normed_all, up_sectioned, preferred_element_type=jnp.float32)  9.06 us
  transfers between devices with their start and end apart: 13, of which 11 were waited for; matrix products, arithmetic and copies ran while one was open for 9% of the time, Pallas kernels for 0%

profile of v1, /device:TPU:0, one launch (start us, length us, event | category | flops | bytes accessed | tf_op | source)
XLA Modules:
  0.0 364.0 jit_solution(15467626486381936391)
XLA Ops:
  8.3 4.9 %collective-permute-start = (bf16[2,128,128]{2,1,0:T(8,128)(2,1)S(1)}, bf16[2,128,128]{2,1,0:T(8,128)(2,1)S(1)}, u32[]{:S(2)}, u32[]{:S(2)}) collective-permute-start(bf16[2,128,128]{2,1,0:T(8,128)(2,1)S(1)} %get-tuple-element.124), channel_id=1, source_target_pairs={{0,4},{4,8},{8,12},{12,16},{16,20},{20,24},{24,28},{1,5},{5,9},{9,... | collective-permute-start | bytes 196616 | tf_op jit(solution)/shard_map/ppermute | solution.py:20
  15.1 4.3 %collective-permute-done.1 = bf16[2,128,128]{2,1,0:T(8,128)(2,1)S(1)} collective-permute-done((bf16[2,128,128]{2,1,0:T(8,128)(2,1)S(1)}, bf16[2,128,128]{2,1,0:T(8,128)(2,1)S(1)}, u32[]{:S(2)}, u32[]{:S(2)}) %collective-permute-start.1) | collective-permute-done | bytes 65568 | tf_op jit(solution)/shard_map/ppermute | solution.py:22
  20.4 10.4 %while.12 = (s32[]{:T(128)}, bf16[2,256,512]{2,1,0:T(8,128)(2,1)}, bf16[2,768,128]{2,1,0:T(8,128)(2,1)S(1)}, s32[2]{0:T(128)S(1)}, s32[]{:T(128)}, /*index=5*/bf...) while((s32[]{:T(128)}, bf16[2,256,512]{2,1,0:T(8,128)(2,1)}, ...), condition=%wide.region_3.4_spmd, body=%wide.region_0.3_spmd.sunk | while | flops 273420544 | bytes 10273660 | solution.py:95
  30.8 3.8 %convolution_convert_fusion.1 = bf16[512,2048]{1,0:T(8,128)(2,1)} fusion(bf16[512,512]{1,0:T(8,128)(2,1)} %bitcast.53, bf16[512,2048]{1,0:T(8,128)(2,1)S(1)} %copy-done), kind=kOutput, calls=%fused_computation.28 | convolution fusion | flops 1074790400 | bytes 4718592 | tf_op jit(solution)/shard_map/dot_general | solution.py:99
  35.8 2.5 collective-permute-start.2
  38.3 23.0 %collective-permute-done.2 = bf16[256,1408]{1,0:T(8,128)(2,1)S(1)} collective-permute-done((bf16[256,1408]{1,0:T(8,128)(2,1)S(1)}, bf16[256,1408]{1,0:T(8,128)(2,1)S(1)}, u32[]{:S(2)}, u32[]{:S(2)}) %collective-permute-start.2) | collective-permute-done | bytes 720928 | tf_op jit(solution)/shard_map/ppermute | solution.py:106
  62.2 2.5 collective-permute-start.3
  64.7 29.3 %collective-permute-done.3 = bf16[256,1408]{1,0:T(8,128)(2,1)S(1)} collective-permute-done((bf16[256,1408]{1,0:T(8,128)(2,1)S(1)}, bf16[256,1408]{1,0:T(8,128)(2,1)S(1)}, u32[]{:S(2)}, u32[]{:S(2)}) %collective-permute-start.3) | collective-permute-done | bytes 720928 | tf_op jit(solution)/shard_map/ppermute | solution.py:106
  95.0 32.6 %collective-permute-done.4 = bf16[256,1408]{1,0:T(8,128)(2,1)S(1)} collective-permute-done((bf16[256,1408]{1,0:T(8,128)(2,1)S(1)}, bf16[256,1408]{1,0:T(8,128)(2,1)S(1)}, u32[]{:S(2)}, u32[]{:S(2)}) %collective-permute-start.4) | collective-permute-done | bytes 720928 | tf_op jit(solution)/shard_map/ppermute | solution.py:106
  128.5 35.0 %collective-permute-done.5 = bf16[256,1408]{1,0:T(8,128)(2,1)S(1)} collective-permute-done((bf16[256,1408]{1,0:T(8,128)(2,1)S(1)}, bf16[256,1408]{1,0:T(8,128)(2,1)S(1)}, u32[]{:S(2)}, u32[]{:S(2)}) %collective-permute-start.5) | collective-permute-done | bytes 720928 | tf_op jit(solution)/shard_map/ppermute | solution.py:106
  164.4 22.0 %collective-permute-done.6 = bf16[256,1408]{1,0:T(8,128)(2,1)S(1)} collective-permute-done((bf16[256,1408]{1,0:T(8,128)(2,1)S(1)}, bf16[256,1408]{1,0:T(8,128)(2,1)S(1)}, u32[]{:S(2)}, u32[]{:S(2)}) %collective-permute-start.6) | collective-permute-done | bytes 720928 | tf_op jit(solution)/shard_map/ppermute | solution.py:106
  187.3 2.1 collective-permute-start.7
  189.4 38.6 %collective-permute-done.7 = bf16[256,1408]{1,0:T(8,128)(2,1)} collective-permute-done((bf16[256,1408]{1,0:T(8,128)(2,1)S(1)}, bf16[256,1408]{1,0:T(8,128)(2,1)}, u32[]{:S(2)}, u32[]{:S(2)}) %collective-permute-start.7) | collective-permute-done | bytes 720928 | tf_op jit(solution)/shard_map/ppermute | solution.py:106
  228.0 5.0 %convert_add_fusion = (f32[512,2048]{1,0:T(8,128)}, f32[512]{0:T(512)S(1)}) fusion(bf16[512,2048]{1,0:T(8,128)(2,1)} %all-reduce.2.cloned.1.call-done, bf16[512,2048]{1,0:T(8,128)(2,1)} %param.16), kind=kLoop, calls=%fused_computation.27 | loop fusion | flops 5242368 | bytes 8390656 | tf_op jit(solution)/shard_map/add | solution.py:101
  233.0 10.3 %collective-permute-done.8 = bf16[256,1408]{1,0:T(8,128)(2,1)} collective-permute-done((bf16[256,1408]{1,0:T(8,128)(2,1)}, bf16[256,1408]{1,0:T(8,128)(2,1)}, u32[]{:S(2)}, u32[]{:S(2)}) %collective-permute-start.8) | collective-permute-done | bytes 720928 | tf_op jit(solution)/shard_map/ppermute | solution.py:106
  243.3 2.0 constant_dynamic-update-slice_fusion.16
  245.4 2.1 constant_dynamic-update-slice_fusion.15
  253.0 2.0 constant_dynamic-update-slice_fusion.8
  255.1 2.0 constant_dynamic-update-slice_fusion.7
  262.7 9.1 %fusion.21 = f32[512,1408]{1,0:T(8,128)} fusion(bf16[2048,1408]{1,0:T(8,128)(2,1)} %all-gather.3.cloned.1.call-done, f32[2048]{0:T(1024)S(1)} %copy-done.13, f32[512]{0:T(512)S(1)} %add_rsqrt_fusion, bf16[512,2048]{1,0:T(8,128)(2,1)} %all-reduce.2.cloned.1.call-done, bf16[512,2048]{1,0:T(8,128)(2,1)} %param.16), kind=kOutput, calls=%fused_computation.54 | convolution fusion | flops 2959081472 | bytes 12855296 | tf_op jit(solution)/shard_map/dot_general | solution.py:112
  271.7 18.7 %all-gather.5.cloned.1.call-done = bf16[1408,2048]{1,0:T(8,128)(2,1)} async-done(((bf16[1408,256]{1,0:T(8,128)(2,1)}), bf16[1408,2048]{1,0:T(8,128)(2,1)}) %all-gather.5.cloned.1.call-update) | async-done | bytes 5767184 | tf_op jit(solution)/shard_map/all_gather | solution.py:61
  290.4 14.6 %convolution_convert_fusion.2 = bf16[512,2048]{1,0:T(8,128)(2,1)} fusion(bf16[1408,2048]{1,0:T(8,128)(2,1)} %all-gather.5.cloned.1.call-done, f32[512,1408]{1,0:T(8,128)} %fusion.21, bf16[4096,1408]{1,0:T(8,128)(2,1)} %constant_dynamic-update-slice_fusion.1, s32[]{:T(128)S(6)} %select_n.38, f32[2048]{0:T(1024)S(1)} %copy-done.13, ...), kind=kOutput, calls=%fused_computation.29 | convolution fusion | flops 5917245440 | bytes 20719620 | tf_op jit(solution)/shard_map/dot_general | solution.py:116
  305.1 49.2 %reduce-scatter.2.cloned.1.call-done = bf16[128,2048]{1,0:T(8,128)(2,1)} async-done(((bf16[512,2048]{1,0:T(8,128)(2,1)}), bf16[128,2048]{1,0:T(8,128)(2,1)}) %reduce-scatter.2.cloned.1.call-update) | async-done | bytes 524304 | tf_op jit(solution)/shard_map/reduce_scatter | solution.py:115
  354.3 2.3 add_convert_fusion
  (93 shorter events, 29.6 us)
Async XLA Ops:
  7.4 23.4 %copy-start = (bf16[512,2048]{1,0:T(8,128)(2,1)S(1)}, bf16[512,2048]{1,0:T(8,128)(2,1)}, u32[]{:S(2)}) copy-start(bf16[512,2048]{1,0:T(8,128)(2,1)} %param.18) | copy-start | bytes 6291460
  7.4 220.6 %all-reduce.2.cloned.1.call-start = ((), (), s32[]{:S(2)}) async-start(), calls=%async_computation.1 | async-start | bytes 4194304 | tf_op jit(solution)/shard_map/psum | solution.py:98
  8.3 6.8 %collective-permute-start = (bf16[2,128,128]{2,1,0:T(8,128)(2,1)S(1)}, bf16[2,128,128]{2,1,0:T(8,128)(2,1)S(1)}, u32[]{:S(2)}, u32[]{:S(2)}) collective-permute-start(bf16[2,128,128]{2,1,0:T(8,128)(2,1)S(1)} %get-tuple-element.124), channel_id=1, source_target_pairs={{0,4},{4,8},{8,12},{12,16},{16,20},{20,24},{24,28},{1,5},{5,9},{9,... | collective-permute-start | bytes 196616 | tf_op jit(solution)/shard_map/ppermute | solution.py:20
  13.2 6.2 %collective-permute-start.1 = (bf16[2,128,128]{2,1,0:T(8,128)(2,1)S(1)}, bf16[2,128,128]{2,1,0:T(8,128)(2,1)S(1)}, u32[]{:S(2)}, u32[]{:S(2)}) collective-permute-start(bf16[2,128,128]{2,1,0:T(8,128)(2,1)S(1)} %get-tuple-element.125), channel_id=1, source_target_pairs={{4,0},{8,4},{12,8},{16,12},{20,16},{24,20},{28,24},{5,1},{9,5},{13... | collective-permute-start | bytes 196616 | tf_op jit(solution)/shard_map/ppermute | solution.py:22
  20.4 3.3 copy-start.12
  25.6 3.3 copy-start.12
  30.8 5.0 %copy-start.1 = (bf16[256,1408]{1,0:T(8,128)(2,1)S(1)}, bf16[256,1408]{1,0:T(8,128)(2,1)}, u32[]{:S(2)}) copy-start(bf16[256,1408]{1,0:T(8,128)(2,1)} %param.19) | copy-start | bytes 2162692
  34.6 228.1 %all-gather.3.cloned.1.call-start = ((), (), s32[]{:S(2)}) async-start(), calls=%async_computation.2 | async-start | bytes 6488064 | tf_op jit(solution)/shard_map/all_gather | solution.py:110
  35.2 255.3 %all-gather.5.cloned.1.call-start = ((), (), s32[]{:S(2)}) async-start(), calls=%async_computation.3 | async-start | bytes 6488064 | tf_op jit(solution)/shard_map/all_gather | solution.py:61
  35.7 318.6 %reduce-scatter.2.cloned.1.call-start = ((), (), s32[]{:S(2)}) async-start(), calls=%async_computation.4 | async-start | bytes 2621440 | tf_op jit(solution)/shard_map/reduce_scatter | solution.py:115
  35.8 25.5 %collective-permute-start.2 = (bf16[256,1408]{1,0:T(8,128)(2,1)S(1)}, bf16[256,1408]{1,0:T(8,128)(2,1)S(1)}, u32[]{:S(2)}, u32[]{:S(2)}) collective-permute-start(bf16[256,1408]{1,0:T(8,128)(2,1)S(1)} %copy-done.1), channel_id=1, source_target_pairs={{0,4},{4,8},{8,12},{12,16},{16,20},{20,24},{24,28},{28,0},{1,5},{5... | collective-permute-start | bytes 2162696 | tf_op jit(solution)/shard_map/ppermute | solution.py:106
  62.2 31.8 %collective-permute-start.3 = (bf16[256,1408]{1,0:T(8,128)(2,1)S(1)}, bf16[256,1408]{1,0:T(8,128)(2,1)S(1)}, u32[]{:S(2)}, u32[]{:S(2)}) collective-permute-start(bf16[256,1408]{1,0:T(8,128)(2,1)S(1)} %collective-permute-done.2), channel_id=1, source_target_pairs={{0,4},{4,8},{8,12},{12,16},{16,20},{20,24},{24,28},{28,0},{1,5},{5... | collective-permute-start | bytes 2162696 | tf_op jit(solution)/shard_map/ppermute | solution.py:106
  94.0 0.9 copy-start.4
  95.0 32.6 %collective-permute-start.4 = (bf16[256,1408]{1,0:T(8,128)(2,1)S(1)}, bf16[256,1408]{1,0:T(8,128)(2,1)S(1)}, u32[]{:S(2)}, u32[]{:S(2)}) collective-permute-start(bf16[256,1408]{1,0:T(8,128)(2,1)S(1)} %collective-permute-done.3), channel_id=1, source_target_pairs={{0,4},{4,8},{8,12},{12,16},{16,20},{20,24},{24,28},{28,0},{1,5},{5... | collective-permute-start | bytes 2162696 | tf_op jit(solution)/shard_map/ppermute | solution.py:106
  128.4 35.0 %collective-permute-start.5 = (bf16[256,1408]{1,0:T(8,128)(2,1)S(1)}, bf16[256,1408]{1,0:T(8,128)(2,1)S(1)}, u32[]{:S(2)}, u32[]{:S(2)}) collective-permute-start(bf16[256,1408]{1,0:T(8,128)(2,1)S(1)} %collective-permute-done.4), channel_id=1, source_target_pairs={{0,4},{4,8},{8,12},{12,16},{16,20},{20,24},{24,28},{28,0},{1,5},{5... | collective-permute-start | bytes 2162696 | tf_op jit(solution)/shard_map/ppermute | solution.py:106
  164.4 22.0 %collective-permute-start.6 = (bf16[256,1408]{1,0:T(8,128)(2,1)S(1)}, bf16[256,1408]{1,0:T(8,128)(2,1)S(1)}, u32[]{:S(2)}, u32[]{:S(2)}) collective-permute-start(bf16[256,1408]{1,0:T(8,128)(2,1)S(1)} %collective-permute-done.5), channel_id=1, source_target_pairs={{0,4},{4,8},{8,12},{12,16},{16,20},{20,24},{24,28},{28,0},{1,5},{5... | collective-permute-start | bytes 2162696 | tf_op jit(solution)/shard_map/ppermute | solution.py:106
  187.3 40.7 %collective-permute-start.7 = (bf16[256,1408]{1,0:T(8,128)(2,1)S(1)}, bf16[256,1408]{1,0:T(8,128)(2,1)}, u32[]{:S(2)}, u32[]{:S(2)}) collective-permute-start(bf16[256,1408]{1,0:T(8,128)(2,1)S(1)} %collective-permute-done.6), channel_id=1, source_target_pairs={{0,4},{4,8},{8,12},{12,16},{16,20},{20,24},{24,28},{28,0},{1,5},{5... | collective-permute-start | bytes 2162696 | tf_op jit(solution)/shard_map/ppermute | solution.py:106
  228.0 15.4 %collective-permute-start.8 = (bf16[256,1408]{1,0:T(8,128)(2,1)}, bf16[256,1408]{1,0:T(8,128)(2,1)}, u32[]{:S(2)}, u32[]{:S(2)}) collective-permute-start(bf16[256,1408]{1,0:T(8,128)(2,1)} %collective-permute-done.7), channel_id=1, source_target_pairs={{0,4},{4,8},{8,12},{12,16},{16,20},{20,24},{24,28},{28,0},{1,5},{5... | collective-permute-start | bytes 2162696 | tf_op jit(solution)/shard_map/ppermute | solution.py:106
  228.0 19.5 %copy-start.11 = (bf16[256,1408]{1,0:T(8,128)(2,1)S(1)}, bf16[256,1408]{1,0:T(8,128)(2,1)}, u32[]{:S(2)}) copy-start(bf16[256,1408]{1,0:T(8,128)(2,1)} %copy-done.10) | copy-start | bytes 2162692
  233.0 15.4 %copy-start.9 = (bf16[256,1408]{1,0:T(8,128)(2,1)S(1)}, bf16[256,1408]{1,0:T(8,128)(2,1)}, u32[]{:S(2)}) copy-start(bf16[256,1408]{1,0:T(8,128)(2,1)} %copy-done.8) | copy-start | bytes 2162692
  233.0 16.3 %copy-start.7 = (bf16[256,1408]{1,0:T(8,128)(2,1)S(1)}, bf16[256,1408]{1,0:T(8,128)(2,1)}, u32[]{:S(2)}) copy-start(bf16[256,1408]{1,0:T(8,128)(2,1)} %copy-done.6) | copy-start | bytes 2162692
  233.0 17.2 %copy-start.5 = (bf16[256,1408]{1,0:T(8,128)(2,1)S(1)}, bf16[256,1408]{1,0:T(8,128)(2,1)}, u32[]{:S(2)}) copy-start(bf16[256,1408]{1,0:T(8,128)(2,1)} %copy-done.4) | copy-start | bytes 2162692
  233.0 18.1 %copy-start.3 = (bf16[256,1408]{1,0:T(8,128)(2,1)S(1)}, bf16[256,1408]{1,0:T(8,128)(2,1)}, u32[]{:S(2)}) copy-start(bf16[256,1408]{1,0:T(8,128)(2,1)} %copy-done.2) | copy-start | bytes 2162692
  257.1 5.6 %copy-start.13 = (f32[2048]{0:T(1024)S(1)}, f32[2048]{0:T(1024)}, u32[]{:S(2)}) copy-start(f32[2048]{0:T(1024)} %param.17) | copy-start | bytes 24580
  (4 other events, 3.6 us)
Sparse Core Ops, SparseCore 0:
  34.7 52.5 all-reduce.1
  305.2 49.0 reduce-scatter.1
Sparse Core Ops, SparseCore 1:
  37.2 132.5 all-gather.2
  171.7 118.7 all-gather.4
